TPU v7x, 32 devices: a whole 2x2x4 slice. The times are simulated.
32 devices in a mesh: fs: 8 (over z, y), tp: 4 (over x, core).
Axes of the slice: x: 2, y: 2, z: 4, core: 2. Of those that a mesh axis runs over, the one named last changes fastest.
Arguments:
- prompt: bfloat16 [6144, 2048], P('fs'), may hold values from -6 to 6
- routes: int32 [6144, 2], P('fs'), may hold values from 0 to 15, all different within a row; in each aligned block of 768 rows (0 to 767, 768 to 1535, ...) at most 192 rows name the same one
- affinity: float32 [6144, 2], P('fs'), may hold values from 0.05 to 1
- norm_gain: float32 [2048], P('fs'), may hold values from 0.1 to 1.9
- gate_master: float32 [16, 2048, 1024], P(None, 'fs', 'tp'), may hold values from -0.125 to 0.125
- up_master: float32 [16, 2048, 1024], P(None, 'fs', 'tp'), may hold values from -0.125 to 0.125
- down_master: float32 [16, 1024, 2048], P(None, 'fs', 'tp'), may hold values from -0.1875 to 0.1875
Outputs:
- mixed: bfloat16 [6144, 2048], P('fs', 'tp')
- gate_weights: bfloat16 [16, 2048, 1024], P('fs', None, 'tp')
- up_weights: bfloat16 [16, 2048, 1024], P('fs', None, 'tp')
- down_weights: bfloat16 [16, 1024, 2048], P('fs', None, 'tp')
Inputs may be any that keep to these rules, and one draw needn't show every extreme that they name: `routes`: each row names 2 different experts. In each aligned block of 768 rows no expert is named more than 192 times, a bound that some block reaches.
All inputs are finite; a program needn't handle non-finite values.
Results may differ from a plain program's by a relative error of at most 0.0086.
Values may be sent and summed in bfloat16 or wider, within the bound.
A program may use at most 128 MiB of HBM per device.

v0:
```python
import jax
import jax.numpy as jnp
from jax import lax
from jax.sharding import PartitionSpec as P

norm_eps = 1e-06


def per_device(prompt, routes, affinity, norm_gain, gate_master, up_master, down_master):
    tp_count = lax.axis_size("tp")
    experts = gate_master.shape[0]
    gain_rows = norm_gain[None, :, None]
    gate_half = (gate_master * gain_rows).astype(jnp.bfloat16)
    up_half = (up_master * gain_rows).astype(jnp.bfloat16)
    down_half = down_master.astype(jnp.bfloat16)
    gate_new, up_new, down_new = (
        lax.all_to_all(gate_half, "fs", split_axis=0, concat_axis=1, tiled=True),
        lax.all_to_all(up_half, "fs", split_axis=0, concat_axis=1, tiled=True),
        lax.all_to_all(down_half, "fs", split_axis=0, concat_axis=1, tiled=True),
    )
    token_count = prompt.shape[0]
    top_count = routes.shape[1]
    model_width = prompt.shape[1]
    capacity = 2 * token_count * top_count // experts
    flat_ids = routes.reshape(-1)
    onehot = (flat_ids[:, None] == jnp.arange(experts, dtype=jnp.int32)[None, :]).astype(jnp.int32)
    slot_rank = jnp.sum(jnp.cumsum(onehot, axis=0) * onehot, axis=1) - 1
    slot_index = flat_ids * capacity + slot_rank
    values = prompt.astype(jnp.float32)
    normed = (
        values * lax.rsqrt(jnp.mean(values * values, axis=-1, keepdims=True) + norm_eps)
    ).astype(jnp.bfloat16)
    column_width = model_width // tp_count
    column_slice = lax.dynamic_slice_in_dim(
        normed, lax.axis_index("tp") * column_width, column_width, 1
    )
    slot_rows = jnp.broadcast_to(
        column_slice[:, None, :], (token_count, top_count, column_width)
    ).reshape(-1, column_width)
    outbox = (
        jnp.zeros((experts * capacity, column_width), jnp.bfloat16).at[slot_index].set(slot_rows)
    )
    received = lax.all_to_all(
        outbox.reshape(experts, capacity, column_width),
        "fs",
        split_axis=0,
        concat_axis=1,
        tiled=True,
    )
    shard_piece = lax.all_gather(received, "tp", axis=2, tiled=True)
    gate_pre = jnp.einsum("erd,edf->erf", shard_piece, gate_new, preferred_element_type=jnp.float32)
    up_pre = jnp.einsum("erd,edf->erf", shard_piece, up_new, preferred_element_type=jnp.float32)
    hidden = (jax.nn.silu(gate_pre) * up_pre).astype(jnp.bfloat16)
    expert_out = jnp.einsum(
        "erf,efd->erd",
        lax.all_gather(hidden, "tp", axis=2, tiled=True),
        down_new,
        preferred_element_type=jnp.float32,
    ).astype(jnp.bfloat16)
    returned = lax.all_to_all(expert_out, "fs", split_axis=1, concat_axis=0, tiled=True)
    picked = returned.reshape(experts * capacity, -1)[slot_index].reshape(
        token_count, top_count, -1
    )
    share = affinity / jnp.sum(affinity, axis=1, keepdims=True)
    mixed_out = jnp.sum(share[:, :, None] * picked.astype(jnp.float32), axis=1).astype(jnp.bfloat16)
    return (mixed_out, gate_new, up_new, down_new)


def solution(mesh):
    in_specs = (
        P("fs", None),
        P("fs", None),
        P("fs", None),
        P("fs"),
        P(None, "fs", "tp"),
        P(None, "fs", "tp"),
        P(None, "fs", "tp"),
    )
    out_specs = (P("fs", "tp"), P("fs", None, "tp"), P("fs", None, "tp"), P("fs", None, "tp"))
    return jax.shard_map(
        per_device, mesh=mesh, in_specs=in_specs, out_specs=out_specs, check_vma=False
    )
```

profile of v0, /device:TPU:29, one launch (start us, length us, event | category | flops | bytes accessed | tf_op | source)
XLA Modules:
  0.0 412.2 jit_solution(1486511476478039766)
XLA Ops:
  7.2 0.0 all-gather.3.cloned.1.call-start
  7.2 0.7 broadcast_multiply_fusion
  7.9 0.9 copy.27
  8.8 0.2 eq.29
  9.0 0.2 eq.25
  9.2 0.0 copy-start.1
  9.2 5.5 %convert_element_type.36 = f32[768,2048]{1,0:T(8,128)} convert(bf16[768,2048]{1,0:T(8,128)(2,1)} %param.7) | non-fusion elementwise | flops 1572864 | bytes 9437184 | tf_op jit(solution)/shard_map/convert_element_type | solution.py:29
  14.8 0.0 copy-done.1
  14.8 0.7 multiply_reduce_fusion
  15.5 0.2 copy.26
  15.7 0.3 mul.65
  15.9 4.5 %reduce-window.6 = s32[16,12,128]{2,1,0:T(8,128)S(1)} reduce-window(s32[16,12,128]{2,1,0:T(8,128)S(1)} %fusion.4, s32[]{:T(128)} %constant.15.clone.1), window={size=1x1x128 pad=0_0x0_0x127_0}, to_apply=%region_1.2 | reduce-window | flops 3121152 | bytes 196612 | tf_op jit(solution)/shard_map/reduce-window
  20.5 0.4 slice_reduce_fusion
  20.9 0.2 reduce-window.9
  21.1 0.1 broadcast_add_fusion
  21.3 1.6 fusion.1
  22.9 0.8 broadcast_in_dim.5
  23.7 2.0 reshape.101
  25.7 8.8 %scatter_custom_fusion = bf16[3072,512]{1,0:T(8,128)(2,1)S(1)} fusion(s32[1536]{0:T(1024)S(1)} %fusion.7, bf16[1536,512]{1,0:T(8,128)(2,1)} %reshape.101, bf16[]{:T(256)} %constant.13.clone.1), kind=kCustom, calls=%fused_computation.11 | custom fusion | bytes 3146240 | tf_op jit(solution)/shard_map/scatter | solution.py:41
  34.6 73.7 %all_to_all.87 = bf16[16,192,512]{2,1,0:T(8,128)(2,1)S(1)} all-to-all(bf16[16,192,512]{2,1,0:T(8,128)(2,1)S(1)} %bitcast.44), channel_id=1, replica_groups=mesh['fs'=8,'tp'=4] {'fs'}, dimensions={0} | all-to-all | bytes 6291456 | tf_op jit(solution)/shard_map/all_to_all | solution.py:43
  108.3 1.9 copy.29
  110.3 0.0 copy-start.5
  110.3 0.0 all-gather.3.cloned.1.call-update
  110.3 0.7 copy-done.5
  111.0 5.8 %multiply_convert_fusion.1 = (bf16[16,256,256]{2,1,0:T(8,128)(2,1)}, bf16[16,256,256]{2,1,0:T(8,128)(2,1)S(1)}) fusion(f32[16,256,256]{2,1,0:T(8,128)} %param.11, f32[256]{0:T(256)S(1)} %copy-done.5, f32[16,256,256]{2,1,0:T(8,128)} %param.12), kind=kLoop, calls=%fused_computation.4 | loop fusion | flops 4194304 | bytes 12583936 | tf_op jit(solution)/shard_map/convert_element_type | solution.py:13
  116.8 51.3 %all_to_all.88 = bf16[16,256,256]{2,1,0:T(8,128)(2,1)} all-to-all(bf16[16,256,256]{2,1,0:T(8,128)(2,1)S(1)} %get-tuple-element.5), channel_id=1, replica_groups=mesh['fs'=8,'tp'=4] {'fs'}, dimensions={0} | all-to-all | bytes 4194304 | tf_op jit(solution)/shard_map/all_to_all | solution.py:18
  168.1 5.4 %all-to-all-start.1 = ((bf16[16,256,256]{2,1,0:T(8,128)(2,1)}), bf16[16,256,256]{2,1,0:T(8,128)(2,1)S(1)}, u32[]{:S(2)}, u32[]{:S(2)}) async-start(bf16[16,256,256]{2,1,0:T(8,128)(2,1)} %get-tuple-element.4), calls=%async_computation.1 | async-start | bytes 4194304 | tf_op jit(solution)/shard_map/all_to_all | solution.py:17
  173.5 0.0 all-gather.5.cloned.1.call-start
  173.5 3.1 copy.31
  176.6 43.5 %all-to-all-done.1 = bf16[16,256,256]{2,1,0:T(8,128)(2,1)S(1)} async-done(((bf16[16,256,256]{2,1,0:T(8,128)(2,1)}), bf16[16,256,256]{2,1,0:T(8,128)(2,1)S(1)}, u32[]{:S(2)}, u32[]{:S(2)}) %all-to-all-start.1) | async-done | bytes 2097184 | tf_op jit(solution)/shard_map/all_to_all | solution.py:17
  220.1 1.5 copy.30
  221.6 0.0 all-gather.3.cloned.1.call-done
  221.6 0.0 copy-start.2
  221.6 0.0 copy-start.6
  221.6 7.2 %fusion.8 = f32[2,1536,256]{2,1,0:T(8,128)S(1)} fusion(bf16[2,1536,2048]{2,1,0:T(8,128)(2,1)} %all-gather.3.cloned.1.call-done, bf16[2,2048,256]{2,1,0:T(8,128)(2,1)} %bitcast.51), kind=kOutput, calls=%fused_computation.28 | convolution fusion | flops 3221225472 | bytes 17825792 | tf_op jit(solution)/shard_map/erd,edf->erf/dot_general | solution.py:51
  228.8 0.0 copy-done.2
  228.8 2.2 copy-done.6
  231.0 5.0 %fusion = bf16[2,1536,256]{2,1,0:T(8,128)(2,1)} fusion(bf16[2,1536,2048]{2,1,0:T(8,128)(2,1)S(1)} %copy-done.6, bf16[2,2048,256]{2,1,0:T(8,128)(2,1)S(1)} %bitcast.50, f32[2,1536,256]{2,1,0:T(8,128)S(1)} %fusion.8), kind=kOutput, calls=%fused_computation.8 | convolution fusion | flops 3225944064 | bytes 19398656 | tf_op jit(solution)/shard_map/erd,edf->erf/dot_general | solution.py:52
  236.1 0.0 all-gather.5.cloned.1.call-update
  236.1 2.5 convert_element_type.41
  238.6 51.3 %all_to_all.89 = bf16[16,128,512]{2,1,0:T(8,128)(2,1)S(1)} all-to-all(bf16[16,128,512]{2,1,0:T(8,128)(2,1)S(1)} %convert_element_type.41), channel_id=1, replica_groups=mesh['fs'=8,'tp'=4] {'fs'}, dimensions={0} | all-to-all | bytes 4194304 | tf_op jit(solution)/shard_map/all_to_all | solution.py:19
  289.8 0.2 copy.32
  290.0 0.0 copy-start.3
  290.1 0.0 all-gather.5.cloned.1.call-done
  290.1 7.3 %convolution_convert_fusion = bf16[2,1536,512]{2,1,0:T(8,128)(2,1)S(1)} fusion(bf16[2,1536,1024]{2,1,0:T(8,128)(2,1)} %all-gather.5.cloned.1.call-done, bf16[2,1024,512]{2,1,0:T(8,128)(2,1)S(1)} %bitcast.53), kind=kOutput, calls=%fused_computation.5 | convolution fusion | flops 3222798336 | bytes 11534336 | tf_op jit(solution)/shard_map/erf,efd->erd/dot_general | solution.py:54
  297.4 0.0 copy-done.3
  297.4 14.5 %copy.33 = bf16[2,1536,512]{2,0,1:T(2,128)(2,1)} copy(bf16[2,1536,512]{2,1,0:T(8,128)(2,1)S(1)} %convolution_convert_fusion) | data formatting | bytes 6291456 | tf_op jit(solution)/shard_map/convert_element_type | solution.py:59
  311.9 0.0 copy-start.4
  311.9 5.6 %all-to-all-start.4 = ((bf16[2,1536,512]{2,0,1:T(2,128)(2,1)}), bf16[2,1536,512]{2,0,1:T(2,128)(2,1)S(1)}, u32[]{:S(2)}, u32[]{:S(2)}) async-start(bf16[2,1536,512]{2,0,1:T(2,128)(2,1)} %copy.33), calls=%async_computation.4 | async-start | bytes 6291456 | tf_op jit(solution)/shard_map/all_to_all | solution.py:60
  317.5 0.0 copy-done.4
  317.5 0.2 copy.25
  317.7 68.8 %all-to-all-done.4 = bf16[2,1536,512]{2,0,1:T(2,128)(2,1)S(1)} async-done(((bf16[2,1536,512]{2,0,1:T(2,128)(2,1)}), bf16[2,1536,512]{2,0,1:T(2,128)(2,1)S(1)}, u32[]{:S(2)}, u32[]{:S(2)}) %all-to-all-start.4) | async-done | bytes 3145760 | tf_op jit(solution)/shard_map/all_to_all | solution.py:60
  386.6 0.0 copy-start
  386.6 1.7 copy-done
  388.2 2.5 copy.34
  390.8 5.4 %gather_fusion = bf16[1536,512]{1,0:T(8,128)(2,1)} fusion(bf16[3072,512]{1,0:T(8,128)(2,1)S(1)} %bitcast.41, s32[2048]{0:T(1024)S(1)} %pad_clamp_fusion), kind=kCustom, calls=%fused_computation | custom fusion | bytes 3151872 | tf_op jit(solution)/shard_map/gather | solution.py:61
  396.2 3.4 reshape.88
  399.6 5.7 %multiply_reduce_fusion.1 = bf16[768,512]{1,0:T(8,128)(2,1)} fusion(f32[768,2,512]{2,1,0:T(2,128)S(1)} %reshape.88, f32[768,2]{1,0:T(8,128)S(1)} %copy.25), kind=kLoop, calls=%fused_computation.7 | loop fusion | flops 1179648 | bytes 3938304 | tf_op jit(solution)/shard_map/reduce_sum | solution.py:65
  (8 shorter events, 0.1 us)
Async XLA Ops:
  7.2 214.4 %all-gather.3.cloned.1.call-start = ((), (), s32[]{:S(2)}) async-start(), calls=%async_computation.5 | async-start | bytes 15728640 | tf_op jit(solution)/shard_map/all_gather | solution.py:50
  9.2 5.6 %copy-start.1 = (bf16[768,2048]{1,0:T(8,128)(2,1)S(1)}, bf16[768,2048]{1,0:T(8,128)(2,1)}, u32[]{:S(2)}) copy-start(bf16[768,2048]{1,0:T(8,128)(2,1)} %param.7) | copy-start | bytes 9437188
  110.3 0.7 copy-start.5
  168.1 52.1 %all-to-all-start.1 = ((bf16[16,256,256]{2,1,0:T(8,128)(2,1)}), bf16[16,256,256]{2,1,0:T(8,128)(2,1)S(1)}, u32[]{:S(2)}, u32[]{:S(2)}) async-start(bf16[16,256,256]{2,1,0:T(8,128)(2,1)} %get-tuple-element.4), calls=%async_computation.1 | async-start | bytes 4194304 | tf_op jit(solution)/shard_map/all_to_all | solution.py:17
  173.5 116.6 %all-gather.5.cloned.1.call-start = ((), (), s32[]{:S(2)}) async-start(), calls=%async_computation.6 | async-start | bytes 7864320 | tf_op jit(solution)/shard_map/all_gather | solution.py:56
  221.6 7.2 %copy-start.2 = (bf16[8,2,256,256]{3,2,0,1:T(8,128)(2,1)S(1)}, bf16[8,2,256,256]{3,2,0,1:T(8,128)(2,1)}, u32[]{:S(2)}) copy-start(bf16[8,2,256,256]{3,2,0,1:T(8,128)(2,1)} %copy.31) | copy-start | bytes 6291460
  221.6 9.4 %copy-start.6 = (bf16[2,1536,2048]{2,1,0:T(8,128)(2,1)S(1)}, bf16[2,1536,2048]{2,1,0:T(8,128)(2,1)}, u32[]{:S(2)}) copy-start(bf16[2,1536,2048]{2,1,0:T(8,128)(2,1)} %all-gather.3.cloned.1.call-done) | copy-start | bytes 37748740
  290.0 7.4 %copy-start.3 = (bf16[8,2,128,512]{3,2,0,1:T(8,128)(2,1)}, bf16[8,2,128,512]{3,2,0,1:T(8,128)(2,1)S(1)}, u32[]{:S(2)}) copy-start(bf16[8,2,128,512]{3,2,0,1:T(8,128)(2,1)S(1)} %copy.32) | copy-start | bytes 6291460
  311.9 5.6 %copy-start.4 = (f32[768,2]{0,1:T(2,128)S(1)}, f32[768,2]{0,1:T(2,128)}, u32[]{:S(2)}) copy-start(f32[768,2]{0,1:T(2,128)} %param.9) | copy-start | bytes 18436
  311.9 74.7 %all-to-all-start.4 = ((bf16[2,1536,512]{2,0,1:T(2,128)(2,1)}), bf16[2,1536,512]{2,0,1:T(2,128)(2,1)S(1)}, u32[]{:S(2)}, u32[]{:S(2)}) async-start(bf16[2,1536,512]{2,0,1:T(2,128)(2,1)} %copy.33), calls=%async_computation.4 | async-start | bytes 6291456 | tf_op jit(solution)/shard_map/all_to_all | solution.py:60
  386.6 1.7 copy-start
Sparse Core Ops, SparseCore 0:
  110.4 83.7 all-gather.2
  236.2 48.3 all-gather.4
where the time goes:
time: 417 us; the launch traced here: 412 us
  blocking collectives  176 us (42%)
  waiting for transfers between devices  112 us (27%)
  local copies, waits for them, and re-layouts  51.1 us (12%)
  other arithmetic  27.5 us (7%)
  matrix products  19.5 us (5%)
  between operations  14.3 us (3%)
  starting transfers between devices  11 us (3%)
    all_to_all x1, blocking collectives, per_device(): lax.all_to_all(outbox.reshape(experts, capacity, column_width), 'fs', spl...  73.7 us
    all_to_all x1, waiting for transfers between devices, per_device(): lax.all_to_all(expert_out, 'fs', split_axis=1, concat_axis=0, tiled=True)  68.8 us
    all_to_all x1, blocking collectives, per_device(): lax.all_to_all(up_half, 'fs', split_axis=0, concat_axis=1, tiled=True)  51.3 us
    all_to_all x1, blocking collectives, per_device(): lax.all_to_all(down_half, 'fs', split_axis=0, concat_axis=1, tiled=True)  51.3 us
    all_to_all x1, waiting for transfers between devices, per_device(): lax.all_to_all(gate_half, 'fs', split_axis=0, concat_axis=1, tiled=True)  43.5 us
    convert_element_type x1, local copies, waits for them, and re-layouts, per_device(): expert_out = jnp.einsum('erf,efd->erd', lax.all_gather(hidden, 'tp', axis...  14.5 us
    scatter x1, local copies, waits for them, and re-layouts, per_device(): jnp.zeros((experts * capacity, column_width), jnp.bfloat16).at[slot_index]  8.85 us
  transfers between devices with their start and end apart: 4, of which 2 were waited for; matrix products, arithmetic and copies ran while one was open for 3% of the time, Pallas kernels for 0%

commit v1 on v0

v1 whole, which is shorter than its diff:
```python
import functools

import jax
import jax.numpy as jnp
from jax import lax
from jax.experimental import pallas as pl
from jax.experimental.pallas import tpu as pltpu
from jax.sharding import PartitionSpec as P

norm_eps = 1e-06
MESH = pl.DeviceIdType.MESH


def remote(src, dst, send_sem, recv_sem, where):
    return pltpu.make_async_remote_copy(
        src_ref=src,
        dst_ref=dst,
        send_sem=send_sem,
        recv_sem=recv_sem,
        device_id=where,
        device_id_type=MESH,
    )


def loop(first, last, body):
    def step(i, carry):
        body(i)
        return carry

    lax.fori_loop(first, last, step, 0)


class Spread:
    def __init__(self, tp, whole, rows_of, width, sems):
        self.chips = tp // 2
        self.me = lax.axis_index("tp")
        self.chip, self.core = self.me // 2, self.me % 2
        self.whole, self.rows_of, self.width = whole, rows_of, width
        self.first_send, self.first_recv, self.relay_send, self.relay_recv = sems

    def greet(self, barrier):
        for hop in range(self.chips):
            pl.semaphore_signal(barrier, inc=1, device_id={"tp": self.target(hop)}, device_id_type=MESH)
        return self.chips

    def target(self, hop):
        if hop == 0:
            return self.chip * 2 + 1 - self.core
        return lax.rem(self.chip + hop, self.chips) * 2 + self.core

    def block(self, chunk, owner):
        return self.whole.at[:, self.rows_of(chunk), pl.ds(pl.multiple_of(owner * self.width, self.width), self.width)]

    def first(self, chunk, hop):
        mine = self.block(chunk, self.me)
        return remote(mine, mine, self.first_send.at[chunk, hop], self.first_recv.at[chunk, hop], {"tp": self.target(hop)})

    def relay(self, chunk, hop):
        owner = lax.rem(self.chip - hop + self.chips, self.chips) * 2 + self.core
        taken = self.block(chunk, owner)
        return remote(taken, taken, self.relay_send.at[chunk, hop], self.relay_recv.at[chunk, hop], {"tp": self.target(0)})

    def start(self, chunk):
        for hop in [*range(1, self.chips), 0]:
            self.first(chunk, hop).start()

    def hand_on(self, chunk):
        for hop in range(1, self.chips):
            self.first(chunk, hop).wait_recv()
            self.relay(chunk, hop).start()

    def finish(self, chunk):
        self.first(chunk, 0).wait_recv()
        for hop in range(self.chips):
            self.first(chunk, hop).wait_send()
        for hop in range(1, self.chips):
            self.relay(chunk, hop).wait()


def spread_sems(n, tp):
    return [pltpu.SemaphoreType.DMA((n, tp // 2))] * 4


def peer(step, n):
    return lax.rem(lax.axis_index("fs") + step, n)


def source(step, n):
    return lax.rem(lax.axis_index("fs") - step + n, n)


class Weights:
    def __init__(self, n, master, gain, out, raw, send, sems):
        self.n, self.master, self.gain, self.out, self.raw, self.send = n, master, gain, out, raw, send
        self.load_sem, self.send_sem, self.recv_sem = sems
        self.keep, self.rows = master.shape[0] // n, master.shape[1]

    def load(self, step):
        return pltpu.make_async_copy(
            self.master.at[pl.ds(peer(step, self.n) * self.keep, self.keep)], self.raw.at[step], self.load_sem.at[step]
        )

    def place(self):
        me = lax.axis_index("fs")
        return self.out.at[:, pl.ds(pl.multiple_of(me * self.rows, self.rows), self.rows), :]

    def copy(self, step):
        return remote(
            self.send.at[step], self.place(), self.send_sem.at[step], self.recv_sem.at[step], {"fs": peer(step, self.n)}
        )

    def own(self):
        return pltpu.make_async_copy(self.send.at[0], self.place(), self.send_sem.at[0])

    def load_all(self):
        for step in [*range(1, self.n), 0]:
            self.load(step).start()

    def cast(self, step):
        self.load(step).wait()
        block = self.raw[step]
        if self.gain is not None:
            block = block * self.gain[...][None]
        self.send[step] = block.astype(jnp.bfloat16)

    def send_all(self):
        self.cast(1)

        def body(step):
            self.cast(step)
            self.copy(step - 1).start()

        loop(2, self.n, body)
        self.cast(0)
        self.copy(self.n - 1).start()
        self.own().start()

    def finish(self):
        self.own().wait()
        loop(1, self.n, lambda step: self.copy(step).wait())


def greet_all(n, spread):
    barrier = pltpu.get_barrier_semaphore()
    for step in range(1, n):
        pl.semaphore_signal(barrier, inc=1, device_id={"fs": peer(step, n)}, device_id_type=MESH)
    amount = spread.greet(barrier)
    pl.semaphore_wait(barrier, n - 1 + amount)


def dispatch_kernel(n, tp, gain, outbox, gate, up, gate_out, up_out, gathered, *refs):
    gate_raw, up_raw, gate_send, up_send, weight_sems, token_send, token_recv = refs[:7]
    keep, (_, capacity, width) = outbox.shape[0] // n, outbox.shape
    me = lax.axis_index("fs")
    parts = [
        Weights(n, gate, gain, gate_out, gate_raw, gate_send, [weight_sems.at[0, i] for i in range(3)]),
        Weights(n, up, gain, up_out, up_raw, up_send, [weight_sems.at[1, i] for i in range(3)]),
    ]

    def rows_of(chunk):
        return pl.ds(pl.multiple_of(source(chunk, n) * capacity, capacity), capacity)

    spread = Spread(tp, gathered, rows_of, width, refs[7:11])
    column = pl.ds(pl.multiple_of(lax.axis_index("tp") * width, width), width)

    def token(step):
        return remote(
            outbox.at[pl.ds(peer(step, n) * keep, keep)],
            gathered.at[:, pl.ds(pl.multiple_of(me * capacity, capacity), capacity), column],
            token_send.at[step],
            token_recv.at[step],
            {"fs": peer(step, n)},
        )

    own = pltpu.make_async_copy(
        outbox.at[pl.ds(me * keep, keep)], spread.block(0, lax.axis_index("tp")), token_send.at[0]
    )
    own.start()
    for part in parts:
        part.load_all()
    greet_all(n, spread)
    loop(1, n, lambda step: token(step).start())
    own.wait()
    spread.start(0)
    for part in parts:
        part.send_all()

    def body(step):
        token(step).wait_recv()
        spread.start(step)
        spread.hand_on(step - 1)

    loop(1, n, body)
    spread.hand_on(n - 1)
    loop(1, n, lambda step: token(step).wait_send())
    loop(0, n, spread.finish)
    for part in parts:
        part.finish()


def weight_shapes(master, n):
    experts, rows, columns = master.shape
    keep = experts // n
    return (
        jax.ShapeDtypeStruct((keep, rows * n, columns), jnp.bfloat16),
        pltpu.VMEM((n, keep, rows, columns), jnp.float32),
        pltpu.VMEM((n, keep, rows, columns), jnp.bfloat16),
    )


def dispatch(gain, outbox, gate, up):
    n, tp = lax.axis_size("fs"), lax.axis_size("tp")
    experts, capacity, width = outbox.shape
    gate_out, gate_raw, gate_send = weight_shapes(gate, n)
    up_out, up_raw, up_send = weight_shapes(up, n)
    inside, anywhere = pl.BlockSpec(memory_space=pltpu.VMEM), pl.BlockSpec(memory_space=pl.ANY)
    return pl.pallas_call(
        functools.partial(dispatch_kernel, n, tp),
        out_shape=[
            gate_out,
            up_out,
            jax.ShapeDtypeStruct((experts // n, n * capacity, width * tp), jnp.bfloat16),
        ],
        in_specs=[inside, inside, anywhere, anywhere],
        out_specs=[anywhere] * 3,
        scratch_shapes=[gate_raw, up_raw, gate_send, up_send]
        + [pltpu.SemaphoreType.DMA((2, 3, n))]
        + [pltpu.SemaphoreType.DMA((n,))] * 2
        + spread_sems(n, tp),
        compiler_params=pltpu.CompilerParams(
            collective_id=0, has_side_effects=True, vmem_limit_bytes=48 * 2**20
        ),
        name="dispatch",
    )(gain[:, None], outbox, gate, up)


def combine_kernel(n, tp, hidden, down, down_out, returned, *refs):
    raw, send, held, whole, out, weight_sems, back_send, back_recv, local_sem = refs[:9]
    keep, rows, width = hidden.shape
    capacity = rows // n
    me = lax.axis_index("fs")
    part = Weights(n, down, None, held, raw, send, [weight_sems.at[i] for i in range(3)])

    def rows_of(chunk):
        return pl.ds(pl.multiple_of(peer(chunk, n) * capacity, capacity), capacity)

    spread = Spread(tp, whole, rows_of, width, refs[9:13])

    def own(chunk):
        return pltpu.make_async_copy(
            hidden.at[:, rows_of(chunk), :], spread.block(chunk, lax.axis_index("tp")), local_sem.at[chunk]
        )

    part.load_all()
    loop(0, n, lambda chunk: own(chunk).start())
    greet_all(n, spread)

    def begin(chunk):
        own(chunk).wait()
        spread.start(chunk)

    loop(0, n, begin)
    part.send_all()
    loop(0, n, spread.hand_on)
    loop(0, n, spread.finish)
    part.finish()
    keeping = pltpu.make_async_copy(held, down_out, local_sem.at[0])
    keeping.start()

    def back(step):
        return remote(
            out.at[step], returned.at[me], back_send.at[step], back_recv.at[step], {"fs": peer(step, n)}
        )

    def multiply(step):
        for e in range(keep):
            out[step, e] = jnp.dot(
                whole[e, rows_of(step), :], held[e], preferred_element_type=jnp.float32
            ).astype(jnp.bfloat16)

    multiply(1)

    def body(step):
        multiply(step)
        back(step - 1).start()

    loop(2, n, body)
    multiply(0)
    back(n - 1).start()
    mine = pltpu.make_async_copy(out.at[0], returned.at[me], back_send.at[0])
    mine.start()
    keeping.wait()
    mine.wait()
    loop(1, n, lambda step: back(step).wait())


def combine(hidden, down):
    n, tp = lax.axis_size("fs"), lax.axis_size("tp")
    keep, rows, width = hidden.shape
    down_out, raw, send = weight_shapes(down, n)
    columns = down.shape[2]
    block = (n, keep, rows // n, columns)
    inside, anywhere = pl.BlockSpec(memory_space=pltpu.VMEM), pl.BlockSpec(memory_space=pl.ANY)
    return pl.pallas_call(
        functools.partial(combine_kernel, n, tp),
        out_shape=[down_out, jax.ShapeDtypeStruct(block, jnp.bfloat16)],
        in_specs=[inside, anywhere],
        out_specs=[anywhere] * 2,
        scratch_shapes=[
            raw,
            send,
            pltpu.VMEM(down_out.shape, jnp.bfloat16),
            pltpu.VMEM((keep, rows, width * tp), jnp.bfloat16),
            pltpu.VMEM(block, jnp.bfloat16),
            pltpu.SemaphoreType.DMA((3, n)),
            pltpu.SemaphoreType.DMA((n,)),
            pltpu.SemaphoreType.DMA((n,)),
            pltpu.SemaphoreType.DMA((n,)),
        ]
        + spread_sems(n, tp),
        compiler_params=pltpu.CompilerParams(
            collective_id=1, has_side_effects=True, vmem_limit_bytes=48 * 2**20
        ),
        name="combine",
    )(hidden, down)


def per_device(prompt, routes, affinity, norm_gain, gate_master, up_master, down_master):
    tp_count = lax.axis_size("tp")
    experts = gate_master.shape[0]
    token_count, model_width = prompt.shape
    top_count = routes.shape[1]
    capacity = 2 * token_count * top_count // experts

    values = prompt.astype(jnp.float32)
    scale = lax.rsqrt(jnp.mean(values * values, axis=-1, keepdims=True) + norm_eps)
    column_width = model_width // tp_count
    columns = lax.dynamic_slice_in_dim(
        prompt, lax.axis_index("tp") * column_width, column_width, 1
    )
    normed = (columns.astype(jnp.float32) * scale).astype(jnp.bfloat16)

    names = jnp.arange(experts, dtype=jnp.int32)
    hits = (routes.T[:, None, :] == names[None, :, None]).astype(jnp.float32)
    named = jnp.sum(hits, axis=0)
    position = jnp.arange(token_count, dtype=jnp.int32)
    earlier = (position[:, None] < position[None, :]).astype(jnp.bfloat16)
    rank = jnp.dot(named.astype(jnp.bfloat16), earlier, preferred_element_type=jnp.float32)
    slot = jnp.where(named > 0, rank, -1.0).astype(jnp.int32)
    share = (affinity / jnp.sum(affinity, axis=1, keepdims=True)).T
    weight = jnp.sum(hits * share[:, None, :], axis=0)

    places = jnp.arange(capacity, dtype=jnp.int32)
    pick = (slot[:, None, :] == places[None, :, None]).astype(jnp.bfloat16)
    outbox = jnp.einsum(
        "ert,td->erd", pick, normed, preferred_element_type=jnp.float32
    ).astype(jnp.bfloat16)

    gate_new, up_new, gathered = dispatch(norm_gain, outbox, gate_master, up_master)
    gate_pre = jnp.einsum("erd,edf->erf", gathered, gate_new, preferred_element_type=jnp.float32)
    up_pre = jnp.einsum("erd,edf->erf", gathered, up_new, preferred_element_type=jnp.float32)
    hidden = (jax.nn.silu(gate_pre) * up_pre).astype(jnp.bfloat16)
    down_new, returned = combine(hidden, down_master)

    spread = jnp.where(
        slot[:, None, :] == places[None, :, None], weight[:, None, :], 0
    ).astype(jnp.bfloat16)
    mixed = lax.dot_general(
        spread.reshape(experts * capacity, token_count),
        returned.reshape(experts * capacity, -1),
        (((0,), (0,)), ((), ())),
        preferred_element_type=jnp.float32,
    ).astype(jnp.bfloat16)
    return (mixed, gate_new, up_new, down_new)


def solution(mesh):
    in_specs = (
        P("fs", None),
        P("fs", None),
        P("fs", None),
        P("fs"),
        P(None, "fs", "tp"),
        P(None, "fs", "tp"),
        P(None, "fs", "tp"),
    )
    out_specs = (P("fs", "tp"), P("fs", None, "tp"), P("fs", None, "tp"), P("fs", None, "tp"))
    return jax.shard_map(
        per_device, mesh=mesh, in_specs=in_specs, out_specs=out_specs, check_vma=False
    )
```

time: 417 us -> 330 us (0.79); the launches traced: 412 us -> 330 us
  Pallas kernels: 0 us -> 294 us
  blocking collectives: 176 us -> 0 us
  waiting for transfers between devices: 112 us -> 0 us
  local copies, waits for them, and re-layouts: 51.1 us -> 4.24 us
  other arithmetic: 27.5 us -> 6.44 us
  between operations: 14.3 us -> 0.72 us
  starting transfers between devices: 11 us -> 0 us
  matrix products: 19.5 us -> 24 us
    pallas_call x0 -> x2, Pallas kernels: none -> 294 us  [the longest x1 164 us: dispatch(): pl.pallas_call(functools.partial(dispatch_kernel, n, tp), out_shape=[gate...]
    all_to_all x3 -> x0, blocking collectives: 176 us -> none  [the longest x1 73.7 us: per_device(): lax.all_to_all(outbox.reshape(experts, capacity, column_width), 'fs', spl...]
    all_to_all x2 -> x0, waiting for transfers between devices: 112 us -> none  [the longest x1 68.8 us: per_device(): lax.all_to_all(expert_out, 'fs', split_axis=1, concat_axis=0, tiled=True)]
    convert_element_type x2 -> x0, local copies, waits for them, and re-layouts: 17.9 us -> none  [the longest x1 14.5 us: per_device(): expert_out = jnp.einsum('erf,efd->erd', lax.all_gather(hidden, 'tp', axis...]
    convert_element_type x5 -> x1, other arithmetic: 15.4 us -> 1.73 us  [per_device(): spread = jnp.where(slot[:, None, :] == places[None, :, None], weight[:, N...]
    all_to_all x2 -> x0, starting transfers between devices: 11 us -> none  [the longest x1 5.57 us: per_device(): lax.all_to_all(expert_out, 'fs', split_axis=1, concat_axis=0, tiled=True)]
    all_to_all x5 -> x0, local copies, waits for them, and re-layouts: 9.22 us -> none  [the longest x1 3.09 us: per_device(): lax.all_to_all(up_half, 'fs', split_axis=0, concat_axis=1, tiled=True)]
    scatter x1 -> x0, local copies, waits for them, and re-layouts: 8.85 us -> none  [per_device(): jnp.zeros((experts * capacity, column_width), jnp.bfloat16).at[slot_index]]
  transfers between devices with their start and end apart: 4 -> 0, of which waited for: 2 -> 0; matrix products, arithmetic and copies ran while one was open for 3% -> 0% of each run, Pallas kernels for 0% -> 0%
where the time goes in v1:
time: 330 us
  Pallas kernels  294 us (89%)
  matrix products  24 us (7%)
  other arithmetic  6.44 us (2%)
  local copies, waits for them, and re-layouts  4.24 us (1%)
    pallas_call x1, Pallas kernels, dispatch(): pl.pallas_call(functools.partial(dispatch_kernel, n, tp), out_shape=[gate...  164 us
    pallas_call x1, Pallas kernels, combine(): pl.pallas_call(functools.partial(combine_kernel, n, tp), out_shape=[down_...  131 us
    dot_general x1, matrix products, per_device(): jnp.einsum('erd,edf->erf', gathered, up_new, preferred_element_type=jnp.f...  8.54 us

profile of v1, /device:TPU:29, one launch (start us, length us, event | category | flops | bytes accessed | tf_op | source)
XLA Modules:
  0.0 329.8 jit_solution(9005631336620998835)
XLA Ops:
  0.6 0.7 reduce_sum.37
  1.3 0.7 divide_bitcast_fusion
  2.0 0.7 convert_reduce_fusion
  2.8 0.2 fusion.6
  3.0 2.6 multiply_reduce_fusion
  5.6 0.0 copy-start
  5.6 5.3 %fusion.4.outbox = bf16[16,192,512]{2,1,0:T(8,128)(2,1)} fusion(s32[16,768]{1,0:T(8,128)S(1)} %fusion.6, f32[768]{0:T(1024)S(1)} %add_rsqrt_fusion, bf16[768,2048]{1,0:T(8,128)(2,1)} %param.7, s32[]{:T(128)S(6)} %select_n.21), kind=kOutput, calls=%fused_computation.9 | convolution fusion | flops 2421030912 | bytes 3984388 | tf_op jit(solution)/shard_map/ert,td->erd/dot_general | solution.py:355
  10.9 0.0 copy-done
  10.9 0.1 copy.12.gain
  11.0 163.9 %dispatch.1 = (bf16[2,2048,256]{2,1,0:T(8,128)(2,1)S(1)}, bf16[2,2048,256]{2,1,0:T(8,128)(2,1)S(1)}, bf16[2,1536,2048]{2,1,0:T(8,128)(2,1)}) custom-call(f32[256,1]{1,0:T(8,128)S(1)} %copy.12.gain, bf16[16,192,512]{2,1,0:T(8,128)(2,1)} %fusion.4.outbox, f32[16,256,256]{2,1,0:T(8,128)} %gate.1, f32[16,256,256]{2,1,0:T(8,128)} %up.1), custom_call_target="tpu_custom_call" | custom-call | tf_op jit(solution)/shard_map/dispatch/pallas_call | solution.py:217
  174.9 6.4 %fusion.13 = f32[2,1536,256]{2,1,0:T(8,128)S(1)} fusion(bf16[2,1536,2048]{2,1,0:T(8,128)(2,1)} %get-tuple-element.9, bf16[2,2048,256]{2,1,0:T(8,128)(2,1)S(1)} %get-tuple-element.21), kind=kOutput, calls=%fused_computation.24 | convolution fusion | flops 3221225472 | bytes 17825792 | tf_op jit(solution)/shard_map/erd,edf->erf/dot_general | solution.py:360
  181.3 8.5 %fusion.2.hidden = bf16[2,1536,256]{2,1,0:T(8,128)(2,1)S(1)} fusion(bf16[2,1536,2048]{2,1,0:T(8,128)(2,1)} %get-tuple-element.9, bf16[2,2048,256]{2,1,0:T(8,128)(2,1)S(1)} %get-tuple-element.22, f32[2,1536,256]{2,1,0:T(8,128)S(1)} %fusion.13), kind=kOutput, calls=%fused_computation.6 | convolution fusion | flops 3225944064 | bytes 19398656 | tf_op jit(solution)/shard_map/erd,edf->erf/dot_general | solution.py:361
  189.9 130.5 %combine.1 = (bf16[2,1024,512]{2,1,0:T(8,128)(2,1)S(1)}, bf16[8,2,192,512]{3,2,1,0:T(8,128)(2,1)}) custom-call(bf16[2,1536,256]{2,1,0:T(8,128)(2,1)S(1)} %fusion.2.hidden, f32[16,128,512]{2,1,0:T(8,128)} %down.1), custom_call_target="tpu_custom_call" | custom-call | tf_op jit(solution)/shard_map/combine/pallas_call | solution.py:304
  320.5 0.0 copy-start.1
  320.5 1.7 select_convert_fusion
  322.2 0.1 copy-done.1
  322.3 3.5 %convolution_convert_fusion = bf16[768,512]{1,0:T(8,128)(2,1)} fusion(bf16[3072,768]{1,0:T(8,128)(2,1)S(1)} %bitcast.15, bf16[3072,512]{1,0:T(8,128)(2,1)S(1)} %bitcast.18), kind=kOutput, calls=%fused_computation.11 | convolution fusion | flops 2416312320 | bytes 8650752 | tf_op jit(solution)/shard_map/dot_general | solution.py:368
  325.8 1.3 copy.16
  327.2 1.3 copy.17
  328.5 1.3 copy.18
  (1 shorter events, 0.0 us)
Async XLA Ops:
  5.6 5.3 %copy-start = (f32[256]{0:T(256)S(1)}, f32[256]{0:T(256)}, u32[]{:S(2)}) copy-start(f32[256]{0:T(256)} %param.10) | copy-start | bytes 3076
  320.5 1.9 copy-start.1

commit v2 on v1

--- a/solution.py
+++ b/solution.py
@@ -234,9 +234,11 @@
     )(gain[:, None], outbox, gate, up)
 
 
-def combine_kernel(n, tp, hidden, down, down_out, returned, *refs):
-    raw, send, held, whole, out, weight_sems, back_send, back_recv, local_sem = refs[:9]
-    keep, rows, width = hidden.shape
+def combine_kernel(n, tp, gathered, gate, up, down, down_out, returned, *refs):
+    raw, send, held, whole, out, taken, gate_in, up_in = refs[:8]
+    weight_sems, back_send, back_recv, local_sem, in_sem = refs[8:13]
+    keep, rows, _ = gathered.shape
+    width = gate.shape[2]
     capacity = rows // n
     me = lax.axis_index("fs")
     part = Weights(n, down, None, held, raw, send, [weight_sems.at[i] for i in range(3)])
@@ -244,24 +246,48 @@
     def rows_of(chunk):
         return pl.ds(pl.multiple_of(peer(chunk, n) * capacity, capacity), capacity)
 
-    spread = Spread(tp, whole, rows_of, width, refs[9:13])
-
-    def own(chunk):
+    spread = Spread(tp, whole, rows_of, width, refs[13:17])
+    column = pl.ds(pl.multiple_of(lax.axis_index("tp") * width, width), width)
+
+    def take(chunk):
         return pltpu.make_async_copy(
-            hidden.at[:, rows_of(chunk), :], spread.block(chunk, lax.axis_index("tp")), local_sem.at[chunk]
+            gathered.at[:, rows_of(chunk), :], taken.at[:, rows_of(chunk), :], in_sem.at[chunk]
         )
 
+    weights = [
+        pltpu.make_async_copy(gate, gate_in, in_sem.at[n]),
+        pltpu.make_async_copy(up, up_in, in_sem.at[n + 1]),
+    ]
+
     part.load_all()
-    loop(0, n, lambda chunk: own(chunk).start())
+    for weight in weights:
+        weight.start()
+    loop(0, n, lambda chunk: take(chunk).start())
     greet_all(n, spread)
-
-    def begin(chunk):
-        own(chunk).wait()
-        spread.start(chunk)
-
-    loop(0, n, begin)
     part.send_all()
-    loop(0, n, spread.hand_on)
+    for weight in weights:
+        weight.wait()
+
+    def produce(chunk):
+        take(chunk).wait()
+        for e in range(keep):
+            block = taken[e, rows_of(chunk), :]
+            gate_pre = jnp.dot(block, gate_in[e], preferred_element_type=jnp.float32)
+            up_pre = jnp.dot(block, up_in[e], preferred_element_type=jnp.float32)
+            hidden = gate_pre / (1.0 + jnp.exp(-gate_pre)) * up_pre
+            whole[e, rows_of(chunk), column] = hidden.astype(jnp.bfloat16)
+
+    def advance(chunk):
+        produce(chunk)
+        spread.start(chunk - 1)
+        spread.hand_on(chunk - 2)
+
+    produce(0)
+    produce(1)
+    spread.start(0)
+    loop(2, n, advance)
+    spread.start(n - 1)
+    loop(n - 2, n, spread.hand_on)
     loop(0, n, spread.finish)
     part.finish()
     keeping = pltpu.make_async_copy(held, down_out, local_sem.at[0])
@@ -294,17 +320,17 @@
     loop(1, n, lambda step: back(step).wait())
 
 
-def combine(hidden, down):
+def combine(gathered, gate, up, down):
     n, tp = lax.axis_size("fs"), lax.axis_size("tp")
-    keep, rows, width = hidden.shape
+    (keep, rows, _), width = gathered.shape, gate.shape[2]
     down_out, raw, send = weight_shapes(down, n)
     columns = down.shape[2]
     block = (n, keep, rows // n, columns)
-    inside, anywhere = pl.BlockSpec(memory_space=pltpu.VMEM), pl.BlockSpec(memory_space=pl.ANY)
+    anywhere = pl.BlockSpec(memory_space=pl.ANY)
     return pl.pallas_call(
         functools.partial(combine_kernel, n, tp),
         out_shape=[down_out, jax.ShapeDtypeStruct(block, jnp.bfloat16)],
-        in_specs=[inside, anywhere],
+        in_specs=[anywhere] * 4,
         out_specs=[anywhere] * 2,
         scratch_shapes=[
             raw,
@@ -312,17 +338,21 @@
             pltpu.VMEM(down_out.shape, jnp.bfloat16),
             pltpu.VMEM((keep, rows, width * tp), jnp.bfloat16),
             pltpu.VMEM(block, jnp.bfloat16),
+            pltpu.VMEM(gathered.shape, jnp.bfloat16),
+            pltpu.VMEM(gate.shape, jnp.bfloat16),
+            pltpu.VMEM(up.shape, jnp.bfloat16),
             pltpu.SemaphoreType.DMA((3, n)),
             pltpu.SemaphoreType.DMA((n,)),
             pltpu.SemaphoreType.DMA((n,)),
             pltpu.SemaphoreType.DMA((n,)),
+            pltpu.SemaphoreType.DMA((n + 2,)),
         ]
         + spread_sems(n, tp),
         compiler_params=pltpu.CompilerParams(
             collective_id=1, has_side_effects=True, vmem_limit_bytes=48 * 2**20
         ),
         name="combine",
-    )(hidden, down)
+    )(gathered, gate, up, down)
 
 
 def per_device(prompt, routes, affinity, norm_gain, gate_master, up_master, down_master):
@@ -357,10 +387,7 @@
     ).astype(jnp.bfloat16)
 
     gate_new, up_new, gathered = dispatch(norm_gain, outbox, gate_master, up_master)
-    gate_pre = jnp.einsum("erd,edf->erf", gathered, gate_new, preferred_element_type=jnp.float32)
-    up_pre = jnp.einsum("erd,edf->erf", gathered, up_new, preferred_element_type=jnp.float32)
-    hidden = (jax.nn.silu(gate_pre) * up_pre).astype(jnp.bfloat16)
-    down_new, returned = combine(hidden, down_master)
+    down_new, returned = combine(gathered, gate_new, up_new, down_master)
 
     spread = jnp.where(
         slot[:, None, :] == places[None, :, None], weight[:, None, :], 0

time: 330 us -> 319 us (0.967)
  matrix products: 24 us -> 9.02 us
    dot_general x2 -> x0, matrix products: 15 us -> none  [the longest x1 8.54 us: per_device(): jnp.einsum('erd,edf->erf', gathered, up_new, preferred_element_type=jnp.f...]
where the time goes in v2:
time: 319 us
  Pallas kernels  296 us (93%)
  matrix products  9.02 us (3%)
  local copies, waits for them, and re-layouts  6.58 us (2%)
  other arithmetic  6.44 us (2%)
    pallas_call x1, Pallas kernels, dispatch(): pl.pallas_call(functools.partial(dispatch_kernel, n, tp), out_shape=[gate...  164 us
    pallas_call x1, Pallas kernels, combine(): pl.pallas_call(functools.partial(combine_kernel, n, tp), out_shape=[down_...  132 us
    unnamed x11, local copies, waits for them, and re-layouts  6.45 us

profile of v2, /device:TPU:29, one launch (start us, length us, event | category | flops | bytes accessed | tf_op | source)
XLA Modules:
  0.0 318.8 jit_solution(15345253532513571530)
XLA Ops:
  0.6 0.7 reduce_sum.37
  1.3 0.7 divide_bitcast_fusion
  2.0 0.7 convert_reduce_fusion
  2.8 0.2 fusion.5
  3.0 2.6 multiply_reduce_fusion
  5.6 0.0 copy-start.2
  5.6 5.3 %fusion.3.outbox = bf16[16,192,512]{2,1,0:T(8,128)(2,1)} fusion(s32[16,768]{1,0:T(8,128)S(1)} %fusion.5, f32[768]{0:T(1024)S(1)} %add_rsqrt_fusion, bf16[768,2048]{1,0:T(8,128)(2,1)} %param.7, s32[]{:T(128)S(6)} %select_n.21), kind=kOutput, calls=%fused_computation.7 | convolution fusion | flops 2421030912 | bytes 3984388 | tf_op jit(solution)/shard_map/ert,td->erd/dot_general | solution.py:385
  10.9 0.0 copy-done.2
  10.9 0.1 copy.12.gain
  11.0 163.9 %dispatch.1 = (bf16[2,2048,256]{2,1,0:T(8,128)(2,1)S(1)}, bf16[2,2048,256]{2,1,0:T(8,128)(2,1)S(1)}, bf16[2,1536,2048]{2,1,0:T(8,128)(2,1)}) custom-call(f32[256,1]{1,0:T(8,128)S(1)} %copy.12.gain, bf16[16,192,512]{2,1,0:T(8,128)(2,1)} %fusion.3.outbox, f32[16,256,256]{2,1,0:T(8,128)} %gate.1, f32[16,256,256]{2,1,0:T(8,128)} %up.1), custom_call_target="tpu_custom_call" | custom-call | tf_op jit(solution)/shard_map/dispatch/pallas_call | solution.py:217
  174.9 0.0 copy-start
  174.9 1.3 copy-done
  176.2 132.2 %combine.1 = (bf16[2,1024,512]{2,1,0:T(8,128)(2,1)S(1)}, bf16[8,2,192,512]{3,2,1,0:T(8,128)(2,1)}) custom-call(bf16[2,1536,2048]{2,1,0:T(8,128)(2,1)} %get-tuple-element.9.gathered, bf16[2,2048,256]{2,1,0:T(8,128)(2,1)S(1)} %get-tuple-element.21.gate, bf16[2,2048,256]{2,1,0:T(8,128)(2,1)} %copy-done, f32[16,128,512]{2,1,0:T(8,128)} %down.1), custom_call_target="tpu_custom_call" | custom-call | tf_op jit(solution)/shard_map/combine/pallas_call | solution.py:330
  308.4 0.0 copy-start.3
  308.4 1.7 select_convert_fusion
  310.2 0.1 copy-done.3
  310.3 3.5 %convolution_convert_fusion = bf16[768,512]{1,0:T(8,128)(2,1)} fusion(bf16[3072,768]{1,0:T(8,128)(2,1)S(1)} %bitcast.11, bf16[3072,512]{1,0:T(8,128)(2,1)S(1)} %bitcast.14), kind=kOutput, calls=%fused_computation.9 | convolution fusion | flops 2416312320 | bytes 8650752 | tf_op jit(solution)/shard_map/dot_general | solution.py:395
  313.8 0.0 copy-start.1
  313.8 1.3 copy.16
  315.1 1.0 copy-done.1
  316.1 1.3 copy.17
  317.5 1.3 copy.18
  (1 shorter events, 0.0 us)
Async XLA Ops:
  5.6 5.3 %copy-start.2 = (f32[256]{0:T(256)S(1)}, f32[256]{0:T(256)}, u32[]{:S(2)}) copy-start(f32[256]{0:T(256)} %param.10) | copy-start | bytes 3076
  174.9 1.3 copy-start
  308.4 1.9 copy-start.3
  313.8 2.3 copy-start.1
